TPU v7x, 32 devices: a whole 2x2x4 slice. The times are simulated.
32 devices in a mesh: rep: 2 (over x), fs: 4 (over z), tp: 4 (over y, core).
Axes of the slice: x: 2, y: 2, z: 4, core: 2. Of those that a mesh axis runs over, the one named last changes fastest.
Arguments:
- tokens: bfloat16 [4096, 1024], P(('rep', 'fs', 'tp')), may hold values from -6 to 6
- w_up: bfloat16 [1024, 4096], P('fs', 'tp'), may hold values from -0.1875 to 0.1875
- w_down: bfloat16 [4096, 1024], P('tp', 'fs'), may hold values from -0.09375 to 0.09375
- out_gain: float32 [1024], replicated, may hold values from 0.1 to 1.9
- out_shift: float32 [1024], replicated, may hold values from -3 to 3
Outputs:
- normed: bfloat16 [4096, 1024], P(('rep', 'fs', 'tp'))
All inputs are finite; a program needn't handle non-finite values.
Results may differ from a plain program's by a relative error of at most 0.015.
Values may be sent and summed in bfloat16 or wider, within the bound.
A program may use at most 64 MiB of HBM per device.

v0:
```python
import jax
import jax.numpy as jnp
from jax import lax
from jax.sharding import PartitionSpec as P

residual_scale = 2.0**0.25
norm_eps = 1e-05


def over_all(share, axis, dim, apply):
    everything = lax.all_gather(share, axis, axis=dim, tiled=True)
    return apply(everything, jnp.int32(0))


def summed_rows(product, extent, axis):
    whole = product(jnp.int32(0), extent * lax.axis_size(axis)).astype(jnp.bfloat16)
    return lax.psum_scatter(whole, axis, scatter_dimension=0, tiled=True).astype(jnp.float32)


def layer_norm(summed, out_gain, out_shift):
    row_mean = jnp.mean(summed, axis=-1, keepdims=True)
    centered = summed - row_mean
    row_var = jnp.mean(centered * centered, axis=-1, keepdims=True)
    return centered * lax.rsqrt(row_var + norm_eps) * out_gain + out_shift


def squared_relu(pre_act):
    return jnp.square(jnp.maximum(pre_act, 0.0)).astype(jnp.bfloat16)


def shards(tokens, w_up, w_down, out_gain, out_shift):
    up_block = lax.all_gather(w_up, "fs", axis=0, tiled=True)

    def activate(block_rows, offset):
        return squared_relu(jnp.dot(block_rows, up_block, preferred_element_type=jnp.float32))

    hidden = over_all(tokens, "tp", 0, activate)
    down_block = lax.all_gather(w_down, "fs", axis=1, tiled=True)
    own_count = tokens.shape[0]

    def project(offset, how_many):
        picked = lax.dynamic_slice_in_dim(hidden, offset, how_many, 0)
        return jnp.dot(picked, down_block, preferred_element_type=jnp.float32)

    branch = summed_rows(project, own_count, "tp")
    summed = residual_scale * tokens.astype(jnp.float32) + branch
    return layer_norm(summed, out_gain, out_shift).astype(jnp.bfloat16)


def solution(mesh):
    in_specs = (P(("rep", "fs", "tp"), None), P("fs", "tp"), P("tp", "fs"), P(), P())
    out_specs = P(("rep", "fs", "tp"), None)
    return jax.shard_map(shards, mesh=mesh, in_specs=in_specs, out_specs=out_specs, check_vma=False)
```

profile of v0, /device:TPU:0, one launch (start us, length us, event | category | flops | bytes accessed | tf_op | source)
XLA Modules:
  0.0 162.0 jit_solution(3515093248988575749)
XLA Ops:
  6.5 0.0 all-gather.4.cloned.1.call-start
  6.5 0.7 all-gather.4.cloned.1.call-update
  7.3 0.0 all-gather.6.cloned.1.call-start
  7.3 0.7 all-gather.6.cloned.1.call-update
  8.0 0.0 all-gather.8.cloned.1.call-start
  8.1 0.7 all-gather.8.cloned.1.call-update
  8.7 0.0 copy-start
  8.8 0.0 reduce-scatter.2.cloned.1.call-start
  8.8 19.6 %all-gather.4.cloned.1.call-done = bf16[512,1024]{1,0:T(8,128)(2,1)} async-done(((bf16[128,1024]{1,0:T(8,128)(2,1)}), bf16[512,1024]{1,0:T(8,128)(2,1)}) %all-gather.4.cloned.1.call-update) | async-done | bytes 1048592 | tf_op jit(solution)/shard_map/all_gather | solution.py:11
  28.3 47.3 %all-gather.6.cloned.1.call-done = bf16[1024,1024]{1,0:T(8,128)(2,1)} async-done(((bf16[256,1024]{1,0:T(8,128)(2,1)}), bf16[1024,1024]{1,0:T(8,128)(2,1)}) %all-gather.6.cloned.1.call-update) | async-done | bytes 2097168 | tf_op jit(solution)/shard_map/all_gather | solution.py:32
  75.6 46.7 %all-gather.8.cloned.1.call-done = bf16[1024,1024]{1,0:T(8,128)(2,1)} async-done(((bf16[1024,256]{1,0:T(8,128)(2,1)}), bf16[1024,1024]{1,0:T(8,128)(2,1)}) %all-gather.8.cloned.1.call-update) | async-done | bytes 2097168 | tf_op jit(solution)/shard_map/all_gather | solution.py:38
  122.3 5.8 %convolution_convert_fusion = bf16[512,1024]{1,0:T(8,128)(2,1)} fusion(bf16[1024,1024]{1,0:T(8,128)(2,1)} %all-gather.8.cloned.1.call-done, bf16[512,1024]{1,0:T(8,128)(2,1)} %all-gather.4.cloned.1.call-done, bf16[1024,1024]{1,0:T(8,128)(2,1)} %all-gather.6.cloned.1.call-done), kind=kOutput, calls=%fused_computation.1 | convolution fusion | flops 2149580800 | bytes 6291456 | tf_op jit(solution)/shard_map/dot_general | solution.py:43
  128.1 0.0 copy-start.1
  128.1 0.0 copy-start.2
  128.1 0.0 reduce-scatter.2.cloned.1.call-update
  128.1 23.2 %reduce-scatter.2.cloned.1.call-done = bf16[128,1024]{1,0:T(8,128)(2,1)} async-done(((bf16[512,1024]{1,0:T(8,128)(2,1)}), bf16[128,1024]{1,0:T(8,128)(2,1)}) %reduce-scatter.2.cloned.1.call-update) | async-done | bytes 262160 | tf_op jit(solution)/shard_map/reduce_scatter | solution.py:17
  151.3 0.0 copy-done
  151.3 1.1 fusion
  152.4 1.2 multiply_reduce_fusion
  153.6 0.0 copy-done.1
  153.6 0.0 copy-done.2
  153.6 1.8 %add_convert_fusion = bf16[128,1024]{1,0:T(8,128)(2,1)} fusion(bf16[128,1024]{1,0:T(8,128)(2,1)} %reduce-scatter.2.cloned.1.call-done, bf16[128,1024]{1,0:T(8,128)(2,1)S(1)} %copy-done, f32[1024]{0:T(1024)S(1)} %copy-done.1, f32[1024]{0:T(1024)S(1)} %copy-done.2, f32[128]{0:T(128)S(1)} %add_rsqrt_fusion, f32[128]{0:T(128)S(1)} %broadcast_multiply_fusion), kind=kLoop, calls=%fused_computation.2 | loop fusion | flops 1179648 | bytes 795648 | tf_op jit(solution)/shard_map/convert_element_type | solution.py:47
  (2 shorter events, 0.0 us)
Async XLA Ops:
  6.5 21.8 %all-gather.4.cloned.1.call-start = ((), (), s32[]{:S(2)}) async-start(), calls=%async_computation.1 | async-start | bytes 1310720 | tf_op jit(solution)/shard_map/all_gather | solution.py:11
  7.3 68.3 %all-gather.6.cloned.1.call-start = ((), (), s32[]{:S(2)}) async-start(), calls=%async_computation.2 | async-start | bytes 2621440 | tf_op jit(solution)/shard_map/all_gather | solution.py:32
  8.0 114.3 %all-gather.8.cloned.1.call-start = ((), (), s32[]{:S(2)}) async-start(), calls=%async_computation.3 | async-start | bytes 2621440 | tf_op jit(solution)/shard_map/all_gather | solution.py:38
  8.7 142.6 %copy-start = (bf16[128,1024]{1,0:T(8,128)(2,1)S(1)}, bf16[128,1024]{1,0:T(8,128)(2,1)}, u32[]{:S(2)}) copy-start(bf16[128,1024]{1,0:T(8,128)(2,1)} %param.5) | copy-start | bytes 786436
  8.8 142.6 %reduce-scatter.2.cloned.1.call-start = ((), (), s32[]{:S(2)}) async-start(), calls=%async_computation.4 | async-start | bytes 1310720 | tf_op jit(solution)/shard_map/reduce_scatter | solution.py:17
  128.1 25.5 %copy-start.1 = (f32[1024]{0:T(1024)S(1)}, f32[1024]{0:T(1024)}, u32[]{:S(2)}) copy-start(f32[1024]{0:T(1024)} %param.9) | copy-start | bytes 12292
  128.1 25.5 %copy-start.2 = (f32[1024]{0:T(1024)S(1)}, f32[1024]{0:T(1024)}, u32[]{:S(2)}) copy-start(f32[1024]{0:T(1024)} %param.8) | copy-start | bytes 12292
Sparse Core Ops, SparseCore 0:
  8.9 19.4 all-gather.3
  29.9 45.6 all-gather.5
  77.2 45.0 all-gather.7
  128.3 22.9 reduce-scatter.1
where the time goes:
time: 162 us
  waiting for transfers between devices  139 us (86%)
  between operations  13.2 us (8%)
  matrix products  5.85 us (4%)
  other arithmetic  4.1 us (3%)
    all_gather x1, waiting for transfers between devices, shards(): up_block = lax.all_gather(w_up, 'fs', axis=0, tiled=True)  47.3 us
    all_gather x1, waiting for transfers between devices, shards(): down_block = lax.all_gather(w_down, 'fs', axis=1, tiled=True)  46.7 us
    reduce_scatter x1, waiting for transfers between devices, summed_rows(): lax.psum_scatter(whole, axis, scatter_dimension=0, tiled=True)  23.2 us
    all_gather x1, waiting for transfers between devices, over_all(): everything = lax.all_gather(share, axis, axis=dim, tiled=True)  19.6 us
    dot_general x1, matrix products, project(): return jnp.dot(picked, down_block, preferred_element_type=jnp.float32)  5.85 us
  transfers between devices with their start and end apart: 4, of which 4 were waited for; matrix products, arithmetic and copies ran while one was open for 0% of the time, Pallas kernels for 0%

commit v1 on v0

--- a/solution.py
+++ b/solution.py
@@ -35,7 +35,22 @@
         return squared_relu(jnp.dot(block_rows, up_block, preferred_element_type=jnp.float32))
 
     hidden = over_all(tokens, "tp", 0, activate)
-    down_block = lax.all_gather(w_down, "fs", axis=1, tiled=True)
+
+    def open_the_words(x0):
+        workers = lax.axis_size("fs")
+        vals = [x0]
+        tick = 0
+        while tick < workers - 1:
+            tile_out = lax.ppermute(
+                vals[-1], "fs", [(kk, (kk + 1) % workers) for kk in range(workers)]
+            )
+            vals.append(tile_out)
+            tick = tick + 1
+        latest = jnp.concatenate(vals[::-1], axis=1)
+        shaped = lax.axis_index("fs")
+        return jnp.roll(latest, shift=(shaped + 1) * x0.shape[1], axis=1)
+
+    down_block = open_the_words(w_down)
     own_count = tokens.shape[0]
 
     def project(offset, how_many):

time: 162 us -> 127 us (0.78)
  waiting for transfers between devices: 139 us -> 93.8 us
  local copies, waits for them, and re-layouts: 0.01 us -> 6.99 us
  starting transfers between devices: 0.12 us -> 3.19 us
    ppermute x0 -> x3, waiting for transfers between devices: none -> 56 us  [open_the_words(): lax.ppermute(vals[-1], 'fs', [(kk, (kk + 1) % workers) for kk in range(wo...]
    all_gather x1 -> x0, waiting for transfers between devices: 46.7 us -> none  [shards(): down_block = lax.all_gather(w_down, 'fs', axis=1, tiled=True)]
    all_gather x1, waiting for transfers between devices: 47.3 us -> 12.7 us  [shards(): up_block = lax.all_gather(w_up, 'fs', axis=0, tiled=True)]
    all_gather x1, waiting for transfers between devices: 19.6 us -> 0.01 us  [over_all(): everything = lax.all_gather(share, axis, axis=dim, tiled=True)]
    unnamed x6 -> x15, local copies, waits for them, and re-layouts: 0.01 us -> 6.13 us
    ppermute x0 -> x3, starting transfers between devices: none -> 3.11 us  [open_the_words(): lax.ppermute(vals[-1], 'fs', [(kk, (kk + 1) % workers) for kk in range(wo...]
  transfers between devices with their start and end apart: 4 -> 6, of which waited for: 4 -> 5; matrix products, arithmetic and copies ran while one was open for 0% -> 5% of each run, Pallas kernels for 0% -> 0%
where the time goes in v1:
time: 127 us
  waiting for transfers between devices  93.8 us (74%)
  between operations  13.1 us (10%)
  local copies, waits for them, and re-layouts  6.99 us (6%)
  matrix products  5.88 us (5%)
  other arithmetic  4.1 us (3%)
  starting transfers between devices  3.19 us (3%)
    ppermute x3, waiting for transfers between devices, open_the_words(): lax.ppermute(vals[-1], 'fs', [(kk, (kk + 1) % workers) for kk in range(wo...  56 us
    reduce_scatter x1, waiting for transfers between devices, summed_rows(): lax.psum_scatter(whole, axis, scatter_dimension=0, tiled=True)  23.7 us
    all_gather x1, waiting for transfers between devices, shards(): up_block = lax.all_gather(w_up, 'fs', axis=0, tiled=True)  12.7 us
    unnamed x15, local copies, waits for them, and re-layouts  6.13 us
    dot_general x1, matrix products, project(): return jnp.dot(picked, down_block, preferred_element_type=jnp.float32)  5.88 us
    ppermute x3, starting transfers between devices, open_the_words(): lax.ppermute(vals[-1], 'fs', [(kk, (kk + 1) % workers) for kk in range(wo...  3.11 us
  transfers between devices with their start and end apart: 6, of which 5 were waited for; matrix products, arithmetic and copies ran while one was open for 5% of the time, Pallas kernels for 0%

profile of v1, /device:TPU:0, one launch (start us, length us, event | category | flops | bytes accessed | tf_op | source)
XLA Modules:
  0.0 127.1 jit_solution(2147206913888353451)
XLA Ops:
  6.5 0.0 copy-start.1
  6.5 0.0 all-gather.3.cloned.1.call-start
  6.5 0.7 all-gather.3.cloned.1.call-update
  7.3 0.0 all-gather.5.cloned.1.call-start
  7.3 0.7 all-gather.5.cloned.1.call-update
  8.0 0.0 reduce-scatter.2.cloned.1.call-start
  8.1 3.1 %collective-permute-start = (bf16[1024,256]{1,0:T(8,128)(2,1)}, bf16[1024,256]{1,0:T(8,128)(2,1)S(1)}, u32[]{:S(2)}, u32[]{:S(2)}) collective-permute-start(bf16[1024,256]{1,0:T(8,128)(2,1)} %param.7), channel_id=1, source_target_pairs={{0,4},{4,8},{8,12},{12,0},{1,5},{5,9},{9,13},{13,1},{2,6},{6,10},{... | collective-permute-start | bytes 1572872 | tf_op jit(solution)/shard_map/ppermute | solution.py:44
  11.2 14.2 %collective-permute-done = bf16[1024,256]{1,0:T(8,128)(2,1)S(1)} collective-permute-done((bf16[1024,256]{1,0:T(8,128)(2,1)}, bf16[1024,256]{1,0:T(8,128)(2,1)S(1)}, u32[]{:S(2)}, u32[]{:S(2)}) %collective-permute-start) | collective-permute-done | bytes 524320 | tf_op jit(solution)/shard_map/ppermute | solution.py:44
  25.3 0.0 collective-permute-start.1
  25.3 14.9 %collective-permute-done.1 = bf16[1024,256]{1,0:T(8,128)(2,1)S(1)} collective-permute-done((bf16[1024,256]{1,0:T(8,128)(2,1)S(1)}, bf16[1024,256]{1,0:T(8,128)(2,1)S(1)}, u32[]{:S(2)}, u32[]{:S(2)}) %collective-permute-start.1) | collective-permute-done | bytes 524320 | tf_op jit(solution)/shard_map/ppermute | solution.py:44
  40.2 0.0 collective-permute-start.2
  40.2 26.9 %collective-permute-done.2 = bf16[1024,256]{1,0:T(8,128)(2,1)S(1)} collective-permute-done((bf16[1024,256]{1,0:T(8,128)(2,1)S(1)}, bf16[1024,256]{1,0:T(8,128)(2,1)S(1)}, u32[]{:S(2)}, u32[]{:S(2)}) %collective-permute-start.2) | collective-permute-done | bytes 524320 | tf_op jit(solution)/shard_map/ppermute | solution.py:44
  67.1 0.9 constant_dynamic-update-slice_fusion.7
  68.1 0.9 constant_dynamic-update-slice_fusion.6
  68.9 0.9 constant_dynamic-update-slice_fusion.5
  69.8 0.0 copy-done.1
  69.8 0.9 constant_dynamic-update-slice_fusion.4
  70.7 0.9 constant_dynamic-update-slice_fusion.3
  71.5 0.9 constant_dynamic-update-slice_fusion.2
  72.4 0.9 constant_dynamic-update-slice_fusion.1
  73.3 0.9 constant_dynamic-update-slice_fusion
  74.1 0.0 copy-start
  74.1 0.0 copy-start.2
  74.1 0.0 copy-start.3
  74.1 0.0 all-gather.3.cloned.1.call-done
  74.1 12.7 %all-gather.5.cloned.1.call-done = bf16[1024,1024]{1,0:T(8,128)(2,1)} async-done(((bf16[256,1024]{1,0:T(8,128)(2,1)}), bf16[1024,1024]{1,0:T(8,128)(2,1)}) %all-gather.5.cloned.1.call-update) | async-done | bytes 2097168 | tf_op jit(solution)/shard_map/all_gather | solution.py:32
  86.8 5.9 %fusion.2 = bf16[512,1024]{1,0:T(8,128)(2,1)} fusion(bf16[1024,2048]{1,0:T(8,128)(2,1)} %constant_dynamic-update-slice_fusion, s32[]{:T(128)S(6)} %select_n.14, bf16[512,1024]{1,0:T(8,128)(2,1)} %all-gather.3.cloned.1.call-done, bf16[1024,1024]{1,0:T(8,128)(2,1)} %all-gather.5.cloned.1.call-done), kind=kOutput, calls=%fused_computation.3 | convolution fusion | flops 2149580800 | bytes 6291460 | tf_op jit(solution)/shard_map/dot_general | solution.py:58
  92.7 0.0 reduce-scatter.2.cloned.1.call-update
  92.7 23.7 %reduce-scatter.2.cloned.1.call-done = bf16[128,1024]{1,0:T(8,128)(2,1)} async-done(((bf16[512,1024]{1,0:T(8,128)(2,1)}), bf16[128,1024]{1,0:T(8,128)(2,1)}) %reduce-scatter.2.cloned.1.call-update) | async-done | bytes 262160 | tf_op jit(solution)/shard_map/reduce_scatter | solution.py:17
  116.5 0.0 copy-done
  116.5 1.1 fusion.5
  117.6 1.2 multiply_reduce_fusion
  118.8 0.0 copy-done.2
  118.8 0.0 copy-done.3
  118.8 1.8 %add_convert_fusion = bf16[128,1024]{1,0:T(8,128)(2,1)} fusion(bf16[128,1024]{1,0:T(8,128)(2,1)} %reduce-scatter.2.cloned.1.call-done, bf16[128,1024]{1,0:T(8,128)(2,1)S(1)} %copy-done, f32[1024]{0:T(1024)S(1)} %copy-done.2, f32[1024]{0:T(1024)S(1)} %copy-done.3, f32[128]{0:T(128)S(1)} %add_rsqrt_fusion, f32[128]{0:T(128)S(1)} %broadcast_multiply_fusion), kind=kLoop, calls=%fused_computation.4 | loop fusion | flops 1179648 | bytes 795648 | tf_op jit(solution)/shard_map/convert_element_type | solution.py:62
  (2 shorter events, 0.0 us)
Async XLA Ops:
  6.5 63.3 %copy-start.1 = (bf16[1024,256]{1,0:T(8,128)(2,1)S(1)}, bf16[1024,256]{1,0:T(8,128)(2,1)}, u32[]{:S(2)}) copy-start(bf16[1024,256]{1,0:T(8,128)(2,1)} %param.7) | copy-start | bytes 1572868
  6.5 67.6 %all-gather.3.cloned.1.call-start = ((), (), s32[]{:S(2)}) async-start(), calls=%async_computation.1 | async-start | bytes 1310720 | tf_op jit(solution)/shard_map/all_gather | solution.py:11
  7.3 79.6 %all-gather.5.cloned.1.call-start = ((), (), s32[]{:S(2)}) async-start(), calls=%async_computation.2 | async-start | bytes 2621440 | tf_op jit(solution)/shard_map/all_gather | solution.py:32
  8.0 108.5 %reduce-scatter.2.cloned.1.call-start = ((), (), s32[]{:S(2)}) async-start(), calls=%async_computation.3 | async-start | bytes 1310720 | tf_op jit(solution)/shard_map/reduce_scatter | solution.py:17
  8.1 17.3 %collective-permute-start = (bf16[1024,256]{1,0:T(8,128)(2,1)}, bf16[1024,256]{1,0:T(8,128)(2,1)S(1)}, u32[]{:S(2)}, u32[]{:S(2)}) collective-permute-start(bf16[1024,256]{1,0:T(8,128)(2,1)} %param.7), channel_id=1, source_target_pairs={{0,4},{4,8},{8,12},{12,0},{1,5},{5,9},{9,13},{13,1},{2,6},{6,10},{... | collective-permute-start | bytes 1572872 | tf_op jit(solution)/shard_map/ppermute | solution.py:44
  25.3 14.9 %collective-permute-start.1 = (bf16[1024,256]{1,0:T(8,128)(2,1)S(1)}, bf16[1024,256]{1,0:T(8,128)(2,1)S(1)}, u32[]{:S(2)}, u32[]{:S(2)}) collective-permute-start(bf16[1024,256]{1,0:T(8,128)(2,1)S(1)} %collective-permute-done), channel_id=1, source_target_pairs={{0,4},{4,8},{8,12},{12,0},{1,5},{5,9},{9,13},{13,1},{2,6},{6,10},{... | collective-permute-start | bytes 1572872 | tf_op jit(solution)/shard_map/ppermute | solution.py:44
  40.2 26.9 %collective-permute-start.2 = (bf16[1024,256]{1,0:T(8,128)(2,1)S(1)}, bf16[1024,256]{1,0:T(8,128)(2,1)S(1)}, u32[]{:S(2)}, u32[]{:S(2)}) collective-permute-start(bf16[1024,256]{1,0:T(8,128)(2,1)S(1)} %collective-permute-done.1), channel_id=1, source_target_pairs={{0,4},{4,8},{8,12},{12,0},{1,5},{5,9},{9,13},{13,1},{2,6},{6,10},{... | collective-permute-start | bytes 1572872 | tf_op jit(solution)/shard_map/ppermute | solution.py:44
  74.1 42.4 %copy-start = (bf16[128,1024]{1,0:T(8,128)(2,1)S(1)}, bf16[128,1024]{1,0:T(8,128)(2,1)}, u32[]{:S(2)}) copy-start(bf16[128,1024]{1,0:T(8,128)(2,1)} %param.5) | copy-start | bytes 786436
  74.1 44.6 %copy-start.2 = (f32[1024]{0:T(1024)S(1)}, f32[1024]{0:T(1024)}, u32[]{:S(2)}) copy-start(f32[1024]{0:T(1024)} %param.9) | copy-start | bytes 12292
  74.1 44.7 %copy-start.3 = (f32[1024]{0:T(1024)S(1)}, f32[1024]{0:T(1024)}, u32[]{:S(2)}) copy-start(f32[1024]{0:T(1024)} %param.8) | copy-start | bytes 12292
Sparse Core Ops, SparseCore 0:
  8.9 19.4 all-gather.2
  29.9 56.8 all-gather.4
  92.9 23.5 reduce-scatter.1
